TPU v7x, 32 devices: a whole 2x2x4 slice. The times are simulated.
32 devices in a mesh: gr: 2 (over x), sp: 8 (over z, y), tp: 2 (over core).
Axes of the slice: x: 2, y: 2, z: 4, core: 2. Of those that a mesh axis runs over, the one named last changes fastest.
Arguments:
- tokens: bfloat16 [8, 1024, 4096], P('gr', 'sp'), parts along dimension 0, may hold values from -6 to 6
- key_weight: bfloat16 [4096, 2048], P('sp', 'tp'), may hold values from -0.09375 to 0.09375
- value_weight: bfloat16 [4096, 2048], P('sp', 'tp'), may hold values from -0.09375 to 0.09375
- log_decay: float32 [32, 8, 1024], P('tp', 'gr', 'sp'), parts along dimension 1, may hold values from -1 to 0, as said below
- new_query: bfloat16 [8, 2048], P('gr', 'tp'), parts along dimension 0, may hold values from -6 to 6
- new_key: bfloat16 [8, 2048], P('gr', 'tp'), parts along dimension 0, may hold values from -24 to 24
- new_value: bfloat16 [8, 2048], P('gr', 'tp'), parts along dimension 0, may hold values from -6 to 6
- step_decay: float32 [32, 8], P('tp', 'gr'), parts along dimension 1, may hold values from -1.5 to -0.05
- norm_gain: float32 [2048], P('tp'), may hold values from 0.1 to 1.9
Outputs:
- state_cache: float32 [512, 32, 64], P('gr', 'tp'), parts along dimension 0
- first_read: bfloat16 [8, 2048], P('gr', 'tp'), parts along dimension 0
There are 2 independent parts, one for each index of `gr`. A program takes and returns all parts, laid end to end along the dimension named above; an argument that names none is the same for every part. Nothing has to cross between parts.
Inputs may be any that keep to these rules, and one draw needn't show every extreme that they name: `log_decay`: every entry is at most zero.
All inputs are finite; a program needn't handle non-finite values.
Results may differ from a plain program's by a relative error of at most 0.0053.
Values may be sent and summed in bfloat16 or wider, within the bound.
A program may use at most 64 MiB of HBM per device.

v0:
```python
import jax
import jax.numpy as jnp
from jax import lax
from jax.sharding import PartitionSpec as P

HEAD_DIM = 64


def entering(x, axis, combine, identity):
    devices, mine = (lax.axis_size(axis), lax.axis_index(axis))
    everything = lax.all_gather(x, axis)
    start = jnp.broadcast_to(jnp.asarray(identity, x.dtype), x.shape)

    def lap(k, before):
        at = devices - 1 - k
        reached = at > mine
        new = combine(before, everything[at])
        return jnp.where(reached, new, before)

    return lax.fori_loop(0, devices, lap, start)


def rotate_half(values, positions):
    half = values.shape[-1] // 2
    inverse = 10000.0 ** (-jnp.arange(half, dtype=jnp.float32) * (2.0 / values.shape[-1]))
    angles = positions[..., None] * inverse
    cosine = jnp.cos(angles)
    sine = jnp.sin(angles)
    first, second = (values[..., :half], values[..., half:])
    return jnp.concatenate(
        [first * cosine - second * sine, second * cosine + first * sine], axis=-1
    )


def add_totals(earlier, later):
    return earlier + later


def shards(
    tokens,
    key_weight,
    value_weight,
    log_decay,
    new_query,
    new_key,
    new_value,
    step_decay,
    norm_gain,
):
    seqs, span, width = tokens.shape
    heads_here = key_weight.shape[1] // HEAD_DIM
    token_rows = tokens.reshape(seqs * span, width)
    whole_keys, whole_values = (
        lax.all_gather(key_weight, "sp", axis=0, tiled=True),
        lax.all_gather(value_weight, "sp", axis=0, tiled=True),
    )
    key_sum = jnp.dot(token_rows, whole_keys, preferred_element_type=jnp.float32)
    value_sum = jnp.dot(token_rows, whole_values, preferred_element_type=jnp.float32)
    key_vectors = (
        lax.optimization_barrier(key_sum.astype(jnp.bfloat16))
        .astype(jnp.float32)
        .reshape(seqs, span, heads_here, HEAD_DIM)
    )
    values = (
        lax.optimization_barrier(value_sum.astype(jnp.bfloat16))
        .astype(jnp.float32)
        .reshape(seqs, span, heads_here, HEAD_DIM)
    )
    devices = lax.axis_size("sp")
    offset = lax.axis_index("sp") * span
    positions = (offset + jnp.arange(span, dtype=jnp.int32)).astype(jnp.float32)
    rkeys = rotate_half(key_vectors, positions[None, :, None]) * HEAD_DIM ** (-0.5)
    totals = jnp.sum(log_decay, axis=-1)
    later_sum = entering(totals, "sp", add_totals, jnp.zeros_like(totals))
    weight = jnp.exp(totals[:, :, None] - jnp.cumsum(log_decay, axis=-1) + later_sum[:, :, None])
    weighted = rkeys * jnp.transpose(weight, (1, 2, 0))[:, :, :, None]
    term = jnp.einsum("stha,sthb->sahb", weighted, values, precision=lax.Precision.HIGHEST)
    term = term.reshape(seqs * HEAD_DIM, heads_here, HEAD_DIM)
    end_pos = jnp.full((seqs, heads_here), float(span * devices), jnp.float32)
    query = rotate_half(new_query.astype(jnp.float32).reshape(seqs, heads_here, HEAD_DIM), end_pos)
    key_new = rotate_half(
        new_key.astype(jnp.float32).reshape(seqs, heads_here, HEAD_DIM), end_pos
    ) * HEAD_DIM ** (-0.5)
    value_new = new_value.astype(jnp.float32).reshape(seqs, heads_here, HEAD_DIM)
    decay_all = jnp.repeat(jnp.exp(step_decay).T, HEAD_DIM, axis=0)
    key_all = jnp.transpose(key_new, (0, 2, 1)).reshape(seqs * HEAD_DIM, heads_here)
    value_all = jnp.repeat(value_new, HEAD_DIM, axis=0)
    summed = lax.psum(term, "sp")
    state_cache = decay_all[:, :, None] * summed + key_all[:, :, None] * value_all
    state_seq = state_cache.reshape(seqs, HEAD_DIM, heads_here, HEAD_DIM)
    raw = jnp.einsum("sha,sahb->shb", query, state_seq, precision=lax.Precision.HIGHEST)
    center = jnp.mean(raw, axis=-1, keepdims=True)
    spread = jnp.mean(jnp.square(raw - center), axis=-1, keepdims=True)
    normed = (raw - center) * lax.rsqrt(spread + 1e-06) * norm_gain.reshape(heads_here, HEAD_DIM)
    first_read = normed.reshape(seqs, heads_here * HEAD_DIM).astype(jnp.bfloat16)
    return (state_cache, first_read)


def solution(mesh):
    placed = (
        P("gr", "sp", None),
        P("sp", "tp"),
        P("sp", "tp"),
        P("tp", "gr", "sp"),
        P("gr", "tp"),
        P("gr", "tp"),
        P("gr", "tp"),
        P("tp", "gr"),
        P("tp"),
    )
    return jax.shard_map(
        shards,
        mesh=mesh,
        in_specs=placed,
        out_specs=(P("gr", "tp", None), P("gr", "tp")),
        check_vma=False,
    )
```

profile of v0, /device:TPU:0, one launch (start us, length us, event | category | flops | bytes accessed | tf_op | source)
XLA Modules:
  0.0 378.3 jit_solution(3645071348651051041)
XLA Ops:
  7.2 0.7 all-gather.7.cloned.1.call-update
  8.0 0.7 all-gather.5.cloned.1.call-update
  9.0 1.1 reduce_window_sum.13
  10.1 28.8 %all-gather.1 = f32[8,16,4]{1,2,0:T(4,128)S(1)} all-gather(f32[1,16,4]{1,2,0:T(4,128)S(1)} %bitcast.52), channel_id=2, replica_groups=mesh['gr'=2,'sp'=8,'tp'=2] {'sp'}, dimensions={0}, use_global_device_ids=true | all-gather | bytes 2304 | tf_op jit(solution)/shard_map/all_gather | solution.py:11
  38.9 0.3 while.16
  39.5 98.0 %all-gather.7.cloned.1.call-done = bf16[4096,1024]{1,0:T(8,128)(2,1)} async-done(((bf16[512,1024]{1,0:T(8,128)(2,1)}), bf16[4096,1024]{1,0:T(8,128)(2,1)}) %all-gather.7.cloned.1.call-update) | async-done | bytes 8388624 | tf_op jit(solution)/shard_map/all_gather | solution.py:54
  137.5 9.1 %convolution_convert_fusion = bf16[512,1024]{1,0:T(8,128)(2,1)S(1)} fusion(bf16[512,4096]{1,0:T(8,128)(2,1)} %bitcast.53, bf16[4096,1024]{1,0:T(8,128)(2,1)} %all-gather.7.cloned.1.call-done), kind=kOutput, calls=%fused_computation.8 | convolution fusion | flops 4295491584 | bytes 13631488 | tf_op jit(solution)/shard_map/dot_general | solution.py:57
  146.6 115.7 %all-gather.5.cloned.1.call-done = bf16[4096,1024]{1,0:T(8,128)(2,1)} async-done(((bf16[512,1024]{1,0:T(8,128)(2,1)}), bf16[4096,1024]{1,0:T(8,128)(2,1)}) %all-gather.5.cloned.1.call-update) | async-done | bytes 8388624 | tf_op jit(solution)/shard_map/all_gather | solution.py:55
  262.3 10.1 %convolution_convert_fusion.1 = bf16[512,1024]{1,0:T(8,128)(2,1)} fusion(bf16[512,4096]{1,0:T(8,128)(2,1)} %bitcast.54, bf16[4096,1024]{1,0:T(8,128)(2,1)} %all-gather.5.cloned.1.call-done), kind=kOutput, calls=%fused_computation.9 | convolution fusion | flops 4295491584 | bytes 13631488 | tf_op jit(solution)/shard_map/dot_general | solution.py:58
  272.4 2.9 reshape.171
  275.4 1.7 copy.30
  277.0 2.9 reshape.158
  279.9 2.1 multiply_subtract_fusion
  282.1 0.6 maximum_multiply_fusion
  282.7 2.1 fusion.5
  284.7 1.4 copy.37
  286.2 2.1 reshape.148
  289.4 1.2 broadcast_in_dim.8
  290.6 1.1 reshape.153
  291.9 73.2 %all-reduce.2.cloned.1.call-done = f32[256,16,64]{0,2,1:T(8,128)} async-done(((f32[256,16,64]{0,2,1:T(8,128)}), f32[256,16,64]{0,2,1:T(8,128)}) %all-reduce.2.cloned.1.call-update) | async-done | bytes 1048592 | tf_op jit(solution)/shard_map/psum | solution.py:88
  365.0 1.4 multiply_add_fusion
  366.4 0.9 reshape.156
  367.3 3.4 fusion.2
  371.1 0.7 convert_element_type.28
  (55 shorter events, 2.2 us)
Async XLA Ops:
  7.2 1.6 copy-start.1
  7.2 130.3 %all-gather.7.cloned.1.call-start = ((), (), s32[]{:S(2)}) async-start(), calls=%async_computation.1 | async-start | bytes 9437184 | tf_op jit(solution)/shard_map/all_gather | solution.py:54
  7.9 254.4 %all-gather.5.cloned.1.call-start = ((), (), s32[]{:S(2)}) async-start(), calls=%async_computation | async-start | bytes 9437184 | tf_op jit(solution)/shard_map/all_gather | solution.py:55
  8.7 356.3 %all-reduce.2.cloned.1.call-start = ((), (), s32[]{:S(2)}) async-start(), calls=%async_computation.2 | async-start | bytes 2097152 | tf_op jit(solution)/shard_map/psum | solution.py:88
  286.2 2.2 copy-start.6
  286.2 2.3 copy-start.5
  286.2 2.5 copy-start.3
  286.2 2.6 copy-start.4
  286.2 3.0 copy-start.2
  366.4 4.3 %copy-start = (f32[256,16,64]{0,2,1:T(8,128)}, f32[256,16,64]{0,2,1:T(8,128)S(1)}, u32[]{:S(2)}) copy-start(f32[256,16,64]{0,2,1:T(8,128)S(1)} %multiply_add_fusion) | copy-start | bytes 3145732
Sparse Core Ops, SparseCore 0:
  10.1 127.3 all-gather.6
  139.6 122.6 all-gather.4
  288.5 76.4 all-reduce.1
where the time goes:
time: 379 us; the launch traced here: 378 us
  waiting for transfers between devices  288 us (76%)
  blocking collectives  28.8 us (8%)
  matrix products  24.7 us (7%)
  local copies, waits for them, and re-layouts  16 us (4%)
  between operations  14 us (4%)
  other arithmetic  6.37 us (2%)
    all_gather x1, waiting for transfers between devices, shards(): lax.all_gather(value_weight, 'sp', axis=0, tiled=True)  116 us
    all_gather x1, waiting for transfers between devices, shards(): lax.all_gather(key_weight, 'sp', axis=0, tiled=True)  98 us
    psum x1, waiting for transfers between devices, shards(): summed = lax.psum(term, 'sp')  73.2 us
    all_gather x1, blocking collectives, entering(): everything = lax.all_gather(x, axis)  28.8 us
    dot_general x1, matrix products, shards(): jnp.dot(token_rows, whole_values, preferred_element_type=jnp.float32)  10.1 us
    dot_general x1, matrix products, shards(): jnp.dot(token_rows, whole_keys, preferred_element_type=jnp.float32)  9.14 us
  transfers between devices with their start and end apart: 3, of which 3 were waited for; matrix products, arithmetic and copies ran while one was open for 4% of the time, Pallas kernels for 0%

commit v1 on v0

--- a/solution.py
+++ b/solution.py
@@ -85,7 +85,7 @@
     decay_all = jnp.repeat(jnp.exp(step_decay).T, HEAD_DIM, axis=0)
     key_all = jnp.transpose(key_new, (0, 2, 1)).reshape(seqs * HEAD_DIM, heads_here)
     value_all = jnp.repeat(value_new, HEAD_DIM, axis=0)
-    summed = lax.psum(term, "sp")
+    summed = jnp.sum(lax.all_gather(term, "sp"), axis=0)
     state_cache = decay_all[:, :, None] * summed + key_all[:, :, None] * value_all
     state_seq = state_cache.reshape(seqs, HEAD_DIM, heads_here, HEAD_DIM)
     raw = jnp.einsum("sha,sahb->shb", query, state_seq, precision=lax.Precision.HIGHEST)

time: 379 us -> 431 us (1.14)
  waiting for transfers between devices: 288 us -> 333 us
  other arithmetic: 6.37 us -> 12.7 us
    all_gather x0 -> x1, waiting for transfers between devices: none -> 118 us  [shards(): summed = jnp.sum(lax.all_gather(term, 'sp'), axis=0)]
    psum x1 -> x0, waiting for transfers between devices: 73.2 us -> none  [shards(): summed = lax.psum(term, 'sp')]
where the time goes in v1:
time: 431 us
  waiting for transfers between devices  333 us (77%)
  blocking collectives  28.8 us (7%)
  matrix products  24.7 us (6%)
  local copies, waits for them, and re-layouts  17 us (4%)
  between operations  14 us (3%)
  other arithmetic  12.7 us (3%)
    all_gather x1, waiting for transfers between devices, shards(): summed = jnp.sum(lax.all_gather(term, 'sp'), axis=0)  118 us
    all_gather x1, waiting for transfers between devices, shards(): lax.all_gather(value_weight, 'sp', axis=0, tiled=True)  116 us
    all_gather x1, waiting for transfers between devices, shards(): lax.all_gather(key_weight, 'sp', axis=0, tiled=True)  98 us
    all_gather x1, blocking collectives, entering(): everything = lax.all_gather(x, axis)  28.8 us
    dot_general x1, matrix products, shards(): jnp.dot(token_rows, whole_values, preferred_element_type=jnp.float32)  10.1 us
    dot_general x1, matrix products, shards(): jnp.dot(token_rows, whole_keys, preferred_element_type=jnp.float32)  9.14 us
  transfers between devices with their start and end apart: 3, of which 3 were waited for; matrix products, arithmetic and copies ran while one was open for 4% of the time, Pallas kernels for 0%

profile of v1, /device:TPU:0, one launch (start us, length us, event | category | flops | bytes accessed | tf_op | source)
XLA Modules:
  0.0 430.9 jit_solution(15031592654156488314)
XLA Ops:
  7.2 0.7 all-gather.8.cloned.1.call-update
  8.0 0.7 all-gather.6.cloned.1.call-update
  9.0 1.1 reduce_window_sum.13
  10.1 28.8 %all-gather.1 = f32[8,16,4]{1,2,0:T(4,128)S(1)} all-gather(f32[1,16,4]{1,2,0:T(4,128)S(1)} %bitcast.53), channel_id=2, replica_groups=mesh['gr'=2,'sp'=8,'tp'=2] {'sp'}, dimensions={0}, use_global_device_ids=true | all-gather | bytes 2304 | tf_op jit(solution)/shard_map/all_gather | solution.py:11
  39.5 98.0 %all-gather.8.cloned.1.call-done = bf16[4096,1024]{1,0:T(8,128)(2,1)} async-done(((bf16[512,1024]{1,0:T(8,128)(2,1)}), bf16[4096,1024]{1,0:T(8,128)(2,1)}) %all-gather.8.cloned.1.call-update) | async-done | bytes 8388624 | tf_op jit(solution)/shard_map/all_gather | solution.py:54
  137.5 9.1 %convolution_convert_fusion = bf16[512,1024]{1,0:T(8,128)(2,1)S(1)} fusion(bf16[512,4096]{1,0:T(8,128)(2,1)} %bitcast.54, bf16[4096,1024]{1,0:T(8,128)(2,1)} %all-gather.8.cloned.1.call-done), kind=kOutput, calls=%fused_computation.9 | convolution fusion | flops 4295491584 | bytes 13631488 | tf_op jit(solution)/shard_map/dot_general | solution.py:57
  146.6 115.7 %all-gather.6.cloned.1.call-done = bf16[4096,1024]{1,0:T(8,128)(2,1)} async-done(((bf16[512,1024]{1,0:T(8,128)(2,1)}), bf16[4096,1024]{1,0:T(8,128)(2,1)}) %all-gather.6.cloned.1.call-update) | async-done | bytes 8388624 | tf_op jit(solution)/shard_map/all_gather | solution.py:55
  262.3 10.1 %convolution_convert_fusion.1 = bf16[512,1024]{1,0:T(8,128)(2,1)} fusion(bf16[512,4096]{1,0:T(8,128)(2,1)} %bitcast.55, bf16[4096,1024]{1,0:T(8,128)(2,1)} %all-gather.6.cloned.1.call-done), kind=kOutput, calls=%fused_computation.10 | convolution fusion | flops 4295491584 | bytes 13631488 | tf_op jit(solution)/shard_map/dot_general | solution.py:58
  272.4 2.9 reshape.169
  275.4 1.7 copy.34
  277.0 2.9 reshape.156
  279.9 2.1 multiply_subtract_fusion
  282.7 2.1 fusion.5
  284.7 1.4 copy.41
  286.2 2.2 all_gather_reshape.3
  289.5 1.2 broadcast_in_dim.8
  290.8 2.1 reshape.152
  292.9 118.3 %all-gather.10.cloned.1.call-done = f32[8,256,16,64]{1,3,2,0:T(8,128)} async-done(((f32[1,256,16,64]{1,3,2,0:T(8,128)}), f32[8,256,16,64]{1,3,2,0:T(8,128)}) %all-gather.10.cloned.1.call-update) | async-done | bytes 8388624 | tf_op jit(solution)/shard_map/all_gather | solution.py:88
  411.2 4.2 reduce_sum.39
  415.4 0.9 reduce_sum.40
  416.3 2.4 multiply_add_fusion
  418.8 3.4 fusion.2
  422.5 0.7 convert_element_type.28
  423.2 1.2 multiply_add_fusion.1
  (59 shorter events, 3.1 us)
Async XLA Ops:
  7.2 1.6 copy-start.2
  7.2 130.3 %all-gather.8.cloned.1.call-start = ((), (), s32[]{:S(2)}) async-start(), calls=%async_computation.1 | async-start | bytes 9437184 | tf_op jit(solution)/shard_map/all_gather | solution.py:54
  7.9 254.4 %all-gather.6.cloned.1.call-start = ((), (), s32[]{:S(2)}) async-start(), calls=%async_computation | async-start | bytes 9437184 | tf_op jit(solution)/shard_map/all_gather | solution.py:55
  8.7 402.6 %all-gather.10.cloned.1.call-start = ((), (), s32[]{:S(2)}) async-start(), calls=%async_computation.2 | async-start | bytes 9437184 | tf_op jit(solution)/shard_map/all_gather | solution.py:88
  286.1 2.3 copy-start.7
  286.2 2.4 copy-start.6
  286.2 2.6 copy-start.4
  286.2 2.7 copy-start.5
  286.2 3.2 copy-start.3
  289.5 3.4 copy-start
  418.8 4.4 %copy-start.1 = (f32[256,16,64]{0,2,1:T(8,128)S(1)}, f32[256,16,64]{0,2,1:T(8,128)}, u32[]{:S(2)}) copy-start(f32[256,16,64]{0,2,1:T(8,128)} %reshape.152) | copy-start | bytes 3145732
Sparse Core Ops, SparseCore 0:
  10.1 127.3 all-gather.7
  139.6 122.6 all-gather.5
  288.5 122.6 all-gather.9
